TPU v7x, 32 devices: a whole 2x2x4 slice. The times are simulated.
32 devices in a mesh: kv: 16 (over z, x, core), tp: 2 (over y).
Axes of the slice: x: 2, y: 2, z: 4, core: 2. Of those that a mesh axis runs over, the one named last changes fastest.
Arguments:
- hidden_in: bfloat16 [4, 1024, 2048], P(None, 'kv'), may hold values from -84 to 84
- w_query: bfloat16 [2048, 1024], P(None, 'tp'), may hold values from -0.125 to 0.125
- w_cmp_key: bfloat16 [2048, 256], P(None, 'tp'), may hold values from -0.125 to 0.125
- w_cmp_value: bfloat16 [2048, 256], P(None, 'tp'), may hold values from -0.8838835 to 0.8838835
- w_sel_key: bfloat16 [2048, 256], P(None, 'tp'), may hold values from -0.125 to 0.125
- w_sel_value: bfloat16 [2048, 256], P(None, 'tp'), may hold values from -0.8838835 to 0.8838835
- w_gate: bfloat16 [2048, 2, 16], replicated, may hold values from -0.125 to 0.125
- cmp_key_in: bfloat16 [2048, 128], replicated, may hold values from -0.125 to 0.125
- cmp_key_out: bfloat16 [128, 64], replicated, may hold values from -0.5 to 0.5
- cmp_value_in: bfloat16 [2048, 128], replicated, may hold values from -0.125 to 0.125
- cmp_value_out: bfloat16 [128, 64], replicated, may hold values from -0.5 to 0.5
- out_gain: float32 [1024], replicated, may hold values from 0.1 to 1.9
- w_out: bfloat16 [1024, 2048], replicated, may hold values from -0.1875 to 0.1875
- seq_lengths: int32 [4], replicated, may hold values from 1 to 1024, 1638 in all
- chosen: int32 [4, 16, 4, 16], P(None, 'kv', 'tp'), may hold values from -1 to 15, as said below
Outputs:
- attended: bfloat16 [4, 1024, 2048], P(None, 'kv', 'tp')
Inputs may be any that keep to these rules, and one draw needn't show every extreme that they name: chosen[s, b, g, 0] is b itself. Every other entry is -1 or a block index below b, and the entries of one list that are not -1 are distinct. For each block index and key group, the entries after the first slot that name that index all lie in the lists of a single sequence.
All inputs are finite; a program needn't handle non-finite values.
Results may differ from a plain program's by a relative error of at most 0.012.
The roundings to bfloat16 on the way count: a program that leaves them out, or rounds other values in their place, can miss the bound.
Values may be sent and summed in bfloat16 or wider, within the bound.
A program may use at most 64 MiB of HBM per device.

v0:
```python
import jax
import jax.numpy as jnp
from jax import lax
from jax.sharding import PartitionSpec as P

HEADS = 16
HEAD_DIM = 64
CMP_STRIDE = 16
CMP_BLOCK = 32
TOPK = 16


theta_base = 500000.0
norm_eps = 1e-06


def rotate(values, positions):
    width = values.shape[-1]
    half = width // 2
    inverse = jnp.exp(
        -jnp.log(jnp.float32(theta_base)) * jnp.arange(0, width, 2).astype(jnp.float32) / width
    )
    angle = positions.astype(jnp.float32)[:, None] * inverse[None, :]
    cosine = jnp.cos(angle)[:, None, :]
    sine = jnp.sin(angle)[:, None, :]
    first = values[..., :half]
    second = values[..., half:]
    return jnp.concatenate(
        [first * cosine - second * sine, second * cosine + first * sine], axis=-1
    )


def masked_weights(scores, valid):
    top = jnp.max(jnp.where(valid, scores, -1e30), axis=-1, keepdims=True)
    expd = jnp.where(valid, jnp.exp(scores - top), 0.0)
    total = jnp.sum(expd, axis=-1, keepdims=True)
    return (expd / jnp.maximum(total, 1.0)).astype(jnp.bfloat16)


def compress(raw, prior, weight_in, weight_out):
    seqs, span, groups, width = raw.shape
    extended = jnp.concatenate([prior, raw], axis=1)
    count = span // CMP_STRIDE
    front = extended[:, :span].reshape(seqs, count, CMP_STRIDE, groups, width)
    back = extended[:, CMP_STRIDE:].reshape(seqs, count, CMP_STRIDE, groups, width)
    window = jnp.concatenate([front, back], axis=2).transpose(0, 1, 3, 2, 4)
    window = window.reshape(seqs * count * groups, CMP_BLOCK * width)
    inner = jax.nn.gelu(jnp.dot(window, weight_in, preferred_element_type=jnp.float32)).astype(
        jnp.bfloat16
    )
    return jnp.dot(inner, weight_out, preferred_element_type=jnp.float32).reshape(
        seqs, count, groups, width
    )


def shards(
    hidden_in,
    w_query,
    w_cmp_key,
    w_cmp_value,
    w_sel_key,
    w_sel_value,
    w_gate,
    cmp_key_in,
    cmp_key_out,
    cmp_value_in,
    cmp_value_out,
    out_gain,
    w_out,
    seq_lengths,
    chosen,
):
    seqs, span, width = hidden_in.shape
    block_list = lax.axis_size("kv")
    place = lax.axis_index("kv")
    column = lax.axis_index("tp")
    local_heads = w_query.shape[1] // HEAD_DIM
    local_groups = w_sel_key.shape[1] // HEAD_DIM
    per_group = local_heads // local_groups
    count = span // CMP_STRIDE
    scale = HEAD_DIM ** (-0.5)
    rows = hidden_in.reshape(seqs * span, width)
    positions = place * span + jnp.arange(span, dtype=jnp.int32)

    def project(weight_matrix, heads):
        return jnp.dot(rows, weight_matrix, preferred_element_type=jnp.float32).reshape(
            seqs, span, heads, HEAD_DIM
        )

    queries = rotate(project(w_query, local_heads), positions).astype(jnp.bfloat16)
    sel_pairs = jnp.concatenate(
        [rotate(project(w_sel_key, local_groups), positions), project(w_sel_value, local_groups)],
        axis=-1,
    ).astype(jnp.bfloat16)
    raw_pairs = jnp.concatenate(
        [project(w_cmp_key, local_groups), project(w_cmp_value, local_groups)], axis=-1
    ).astype(jnp.bfloat16)
    prior = jnp.zeros((seqs, CMP_STRIDE, local_groups, HEAD_DIM), jnp.bfloat16)
    ends = place * span + jnp.arange(count, dtype=jnp.int32) * CMP_STRIDE + CMP_STRIDE - 1
    cmp_keys = rotate(compress(raw_pairs[..., :HEAD_DIM], prior, cmp_key_in, cmp_key_out), ends)
    cmp_values = compress(raw_pairs[..., HEAD_DIM:], prior, cmp_value_in, cmp_value_out)
    cmp_piece = jnp.concatenate(
        [cmp_keys.astype(jnp.bfloat16), cmp_values.astype(jnp.bfloat16)], axis=-1
    )[:, None]
    picks = chosen[:, 0]
    every_list = lax.all_gather(picks[None, :, :, 1:], "kv", axis=0, tiled=True)
    named = jnp.any(every_list == place, axis=(0, 3)).astype(jnp.int32)
    seq_ids = jnp.arange(seqs, dtype=jnp.int32)[:, None]
    exported_seq = jnp.sum(named * seq_ids, axis=0)
    selector = seq_ids == exported_seq[None, :]
    export = jnp.sum(
        jnp.where(selector[:, None, :, None], sel_pairs, jnp.zeros((), jnp.bfloat16)), axis=0
    )
    export = export[None]
    remote_pairs, remote_entries = (
        lax.all_gather(export, "kv", axis=0, tiled=True),
        lax.all_gather(cmp_piece, "kv", axis=1, tiled=True),
    )
    gate_all = jnp.dot(rows, w_gate.reshape(width, 2 * HEADS), preferred_element_type=jnp.float32)
    gate_all = gate_all.reshape(seqs, span, 2, HEADS)
    gates = jax.nn.sigmoid(lax.dynamic_slice_in_dim(gate_all, column * local_heads, local_heads, 3))
    entry = jnp.arange(block_list * count, dtype=jnp.int32)
    entry_end = entry * CMP_STRIDE + CMP_STRIDE - 1
    cmp_valid = ((entry >= 1)[None, :] & (entry_end[None, :] <= positions[:, None]))[None, None]
    key_pos = jnp.arange(span, dtype=jnp.int32)
    own_valid = key_pos[None, :] <= key_pos[:, None]

    def one_sequence(args):
        seq_queries, seq_entries, seq_picks, seq_pairs, seq_gates, seq_length = args
        block_q = seq_queries.reshape(span, local_groups, per_group, HEAD_DIM)
        entries = seq_entries.reshape(block_list * count, local_groups, 2 * HEAD_DIM)
        scores = (
            jnp.einsum(
                "qghd,egd->ghqe",
                block_q,
                entries[..., :HEAD_DIM],
                preferred_element_type=jnp.float32,
            )
            * scale
        )
        weights = masked_weights(scores, cmp_valid)
        cmp_out = jnp.einsum(
            "ghqe,egd->qghd", weights, entries[..., HEAD_DIM:], preferred_element_type=jnp.float32
        )
        far = jnp.maximum(seq_picks[:, 1:], 0)
        fetched = jax.vmap(lambda table, index: table[index], in_axes=(2, 0))(remote_pairs, far)
        near = jnp.transpose(seq_pairs, (1, 0, 2))[:, None]
        pairs = jnp.concatenate([near, fetched], axis=1).reshape(
            local_groups, TOPK * span, 2 * HEAD_DIM
        )
        far_live = jnp.broadcast_to(
            (seq_picks[:, 1:] >= 0)[:, None, :, None], (local_groups, span, TOPK - 1, span)
        )
        near_live = jnp.broadcast_to(own_valid[None, :, None, :], (local_groups, span, 1, span))
        sel_valid = jnp.concatenate([near_live, far_live], axis=2).reshape(
            local_groups, 1, span, TOPK * span
        )
        scores_s = (
            jnp.einsum(
                "qghd,gmd->ghqm", block_q, pairs[..., :HEAD_DIM], preferred_element_type=jnp.float32
            )
            * scale
        )
        weights_s = masked_weights(scores_s, sel_valid)
        sel_out = jnp.einsum(
            "ghqm,gmd->qghd", weights_s, pairs[..., HEAD_DIM:], preferred_element_type=jnp.float32
        )
        split = seq_gates.reshape(span, 2, local_groups, per_group, 1)
        mixed = split[:, 0] * cmp_out + split[:, 1] * sel_out
        mixed = jnp.where((positions < seq_length)[:, None, None, None], mixed, 0.0)
        return mixed.reshape(span, local_heads * HEAD_DIM).astype(jnp.bfloat16)

    mixed = lax.map(one_sequence, (queries, remote_entries, picks, sel_pairs, gates, seq_lengths))
    mixed = mixed.reshape(seqs * span, local_heads * HEAD_DIM)
    out_width = width // lax.axis_size("tp")
    own_columns = lax.dynamic_slice_in_dim(w_out, column * out_width, out_width, 1)
    piece_wide = lax.all_gather(mixed, "tp", axis=1, tiled=True).astype(jnp.float32)
    scaled_piece = (piece_wide * out_gain[None, :]).astype(jnp.bfloat16)
    total = jnp.dot(scaled_piece, own_columns, preferred_element_type=jnp.float32)
    squares = jnp.sum(piece_wide * piece_wide, axis=-1)
    row_scale = lax.rsqrt(squares / (HEADS * HEAD_DIM) + norm_eps)
    return (total * row_scale[:, None]).astype(jnp.bfloat16).reshape(seqs, span, out_width)


def solution(mesh):
    placed = (
        P(None, "kv", None),
        P(None, "tp"),
        P(None, "tp"),
        P(None, "tp"),
        P(None, "tp"),
        P(None, "tp"),
        P(),
        P(),
        P(),
        P(),
        P(),
        P(),
        P(),
        P(),
        P(None, "kv", "tp", None),
    )
    return jax.shard_map(
        shards, mesh=mesh, in_specs=placed, out_specs=P(None, "kv", "tp"), check_vma=False
    )
```

profile of v0, /device:TPU:0, one launch (start us, length us, event | category | flops | bytes accessed | tf_op | source)
XLA Modules:
  0.0 139.8 jit_solution(10767838875273096668)
XLA Ops:
  0.2 1.3 copy.65
  1.5 0.7 fusion.52
  2.6 23.3 %all-gather.1 = s32[64,2,15]{2,1,0:T(2,128)S(1)} all-gather(s32[4,2,15]{2,1,0:T(2,128)S(1)} %slice.87), channel_id=3, replica_groups=mesh['kv'=16,'tp'=2] {'kv'}, dimensions={0}, use_global_device_ids=true | all-gather | bytes 8160 | tf_op jit(solution)/shard_map/all_gather | solution.py:106
  25.9 1.2 compare_reduce_fusion
  28.2 18.9 %all-gather.2 = bf16[1024,2,128]{2,0,1:T(8,128)(2,1)S(1)} all-gather(bf16[64,2,128]{2,0,1:T(8,128)(2,1)S(1)} %get-tuple-element.167), channel_id=4, replica_groups=mesh['kv'=16,'tp'=2] {'kv'}, dimensions={0}, use_global_device_ids=true | all-gather | bytes 557056 | tf_op jit(solution)/shard_map/all_gather | solution.py:116
  47.2 1.0 copy.55
  48.2 1.8 %convolution_convert_fusion.2 = bf16[4,64,2,64]{1,3,2,0:T(8,128)(2,1)S(1)} fusion(bf16[2,64,2048,1]{2,1,0,3:T(8,128)(2,1)} %bitcast.227, bf16[4,64,2048]{2,1,0:T(8,128)(2,1)S(1)} %copy-done), kind=kOutput, calls=%fused_computation.71 | convolution fusion | flops 134250496 | bytes 1638400 | tf_op jit(solution)/shard_map/dot_general | solution.py:86
  51.1 1.2 copy.59
  52.4 0.7 convolution_convert_fusion.1
  54.3 19.1 %all-gather = bf16[4,64,2,128]{3,2,1,0:T(2,128)(2,1)S(1)} all-gather(bf16[4,4,2,128]{3,2,1,0:T(2,128)(2,1)S(1)} %pad_maximum_fusion.3), channel_id=2, replica_groups=mesh['kv'=16,'tp'=2] {'kv'}, dimensions={1}, use_global_device_ids=true | all-gather | bytes 139264 | tf_op jit(solution)/shard_map/all_gather | solution.py:117
  73.5 0.7 copy.63
  74.1 4.0 %copy.64 = bf16[2048,512]{0,1:T(8,128)(2,1)} copy(bf16[2048,512]{1,0:T(8,128)(2,1)} %param.18) | data formatting | bytes 4194304 | tf_op args[1]
  78.1 2.8 %fusion.54 = f32[4,64,8,64]{1,3,2,0:T(8,128)S(1)} fusion(bf16[8,64,2048,1]{2,1,0,3:T(8,128)(2,1)} %bitcast.222, bf16[4,64,2048]{2,1,0:T(8,128)(2,1)S(1)} %copy-done), kind=kOutput, calls=%fused_computation.78 | convolution fusion | flops 536870912 | bytes 3670016 | tf_op jit(solution)/shard_map/dot_general | solution.py:86
  83.1 43.9 %while.11 = (s32[]{:T(128)}, bf16[4,64,512]{2,1,0:T(8,128)(2,1)}, s32[4]{0:T(128)}, f32[4,64,2,8]{1,3,2,0:T(8,128)}, bf16[4,16,4,2,128]{4,2,1,3,0:T(4,128)(2,1)}...) while((s32[]{:T(128)}, bf16[4,64,512]{2,1,0:T(8,128)(2,1)}, ...), condition=%wide.region_8.9_spmd.clone, body=%wide.region_3.8_spmd.clone.sunk | while | flops 147700704 | bytes 25832684 | solution.py:173
  83.3 0.7 gather_fusion
  84.2 0.7 copy-done.1
  86.0 1.1 broadcast_in_dim.207
  87.1 1.8 %fusion.134 = (f32[2,4,64]{2,1,0:T(4,128)S(1)}, f32[2,4,64,1024]{3,2,1,0:T(8,128)S(1)}) fusion(f32[2,1024,64,4]{1,2,3,0:T(8,128)S(1)} %fusion.133, pred[2,64,1024]{2,1,0:T(8,128)(4,1)} %broadcast_in_dim.207), kind=kOutput, calls=%fused_computation.151.clone.1 | output fusion | flops 3146751 | bytes 4327424 | tf_op jit(solution)/shard_map/while/body/eval_jaxpr/sub | solution.py:35
  88.9 0.7 constant_dynamic-slice_fusion.8
  89.6 0.9 fusion.135
  90.5 0.9 constant_dynamic-slice_fusion.9
  92.4 0.7 add_compare_fusion.2
  94.3 0.7 gather_fusion
  95.2 0.7 copy-done.1
  97.0 1.1 broadcast_in_dim.207
  98.0 1.8 %fusion.134 = (f32[2,4,64]{2,1,0:T(4,128)S(1)}, f32[2,4,64,1024]{3,2,1,0:T(8,128)S(1)}) fusion(f32[2,1024,64,4]{1,2,3,0:T(8,128)S(1)} %fusion.133, pred[2,64,1024]{2,1,0:T(8,128)(4,1)} %broadcast_in_dim.207), kind=kOutput, calls=%fused_computation.151.clone.1 | output fusion | flops 3146751 | bytes 4327424 | tf_op jit(solution)/shard_map/while/body/eval_jaxpr/sub | solution.py:35
  99.8 0.7 constant_dynamic-slice_fusion.8
  100.6 0.9 fusion.135
  101.5 0.9 constant_dynamic-slice_fusion.9
  103.4 0.7 add_compare_fusion.2
  105.3 0.7 gather_fusion
  106.2 0.7 copy-done.1
  107.9 1.1 broadcast_in_dim.207
  109.0 1.8 %fusion.134 = (f32[2,4,64]{2,1,0:T(4,128)S(1)}, f32[2,4,64,1024]{3,2,1,0:T(8,128)S(1)}) fusion(f32[2,1024,64,4]{1,2,3,0:T(8,128)S(1)} %fusion.133, pred[2,64,1024]{2,1,0:T(8,128)(4,1)} %broadcast_in_dim.207), kind=kOutput, calls=%fused_computation.151.clone.1 | output fusion | flops 3146751 | bytes 4327424 | tf_op jit(solution)/shard_map/while/body/eval_jaxpr/sub | solution.py:35
  110.8 0.7 constant_dynamic-slice_fusion.8
  111.5 0.9 fusion.135
  112.5 0.9 constant_dynamic-slice_fusion.9
  114.3 0.7 add_compare_fusion.2
  116.3 0.7 gather_fusion
  117.1 0.7 copy-done.1
  118.9 1.1 broadcast_in_dim.207
  120.0 1.8 %fusion.134 = (f32[2,4,64]{2,1,0:T(4,128)S(1)}, f32[2,4,64,1024]{3,2,1,0:T(8,128)S(1)}) fusion(f32[2,1024,64,4]{1,2,3,0:T(8,128)S(1)} %fusion.133, pred[2,64,1024]{2,1,0:T(8,128)(4,1)} %broadcast_in_dim.207), kind=kOutput, calls=%fused_computation.151.clone.1 | output fusion | flops 3146751 | bytes 4327424 | tf_op jit(solution)/shard_map/while/body/eval_jaxpr/sub | solution.py:35
  121.8 0.7 constant_dynamic-slice_fusion.8
  122.5 0.9 fusion.135
  123.5 0.9 constant_dynamic-slice_fusion.9
  125.3 0.7 add_compare_fusion.2
  127.0 9.4 %all_gather.15 = bf16[256,1024]{1,0:T(8,128)(2,1)S(1)} all-gather(bf16[256,512]{1,0:T(8,128)(2,1)} %bitcast.233), channel_id=1, replica_groups=mesh['kv'=16,'tp'=2] {'tp'}, dimensions={1}, use_global_device_ids=true | all-gather | bytes 786432 | tf_op jit(solution)/shard_map/all_gather | solution.py:177
  136.7 3.1 %fusion.46 = bf16[256,1024]{1,0:T(8,128)(2,1)} fusion(bf16[1024,2048]{1,0:T(8,128)(2,1)} %param.29, s32[]{:T(128)S(6)} %select_n.31, bf16[256,1024]{1,0:T(8,128)(2,1)S(1)} %all_gather.15, f32[256]{0:T(256)S(1)} %add_rsqrt_fusion, f32[1024]{0:T(1024)} %param.28), kind=kOutput, calls=%fused_computation.68 | convolution fusion | flops 538181632 | bytes 3150852 | tf_op jit(solution)/shard_map/dot_general | solution.py:179
  (215 shorter events, 19.6 us)
Async XLA Ops:
  0.0 1.5 %copy-start = (bf16[4,64,2048]{2,1,0:T(8,128)(2,1)S(1)}, bf16[4,64,2048]{2,1,0:T(8,128)(2,1)}, u32[]{:S(2)}) copy-start(bf16[4,64,2048]{2,1,0:T(8,128)(2,1)} %param.17) | copy-start | bytes 3145732
  0.0 2.5 %copy-start.14 = (s32[4,1,2,16]{3,2,1,0:T(2,128)S(1)}, s32[4,1,2,16]{3,2,1,0:T(2,128)}, u32[]{:S(2)}) copy-start(s32[4,1,2,16]{3,2,1,0:T(2,128)} %param.31) | copy-start | bytes 1540
  0.0 27.3 %copy-start.9 = (bf16[2048,128]{1,0:T(8,128)(2,1)S(1)}, bf16[2048,128]{1,0:T(8,128)(2,1)}, u32[]{:S(2)}) copy-start(bf16[2048,128]{1,0:T(8,128)(2,1)} %param.22) | copy-start | bytes 1572868
  25.9 21.3 %copy-start.10 = (bf16[2048,128]{1,0:T(8,128)(2,1)S(1)}, bf16[2048,128]{1,0:T(8,128)(2,1)}, u32[]{:S(2)}) copy-start(bf16[2048,128]{1,0:T(8,128)(2,1)} %param.19) | copy-start | bytes 1572868
  48.2 2.5 %copy-start.11 = (bf16[2048,128]{1,0:T(8,128)(2,1)S(1)}, bf16[2048,128]{1,0:T(8,128)(2,1)}, u32[]{:S(2)}) copy-start(bf16[2048,128]{1,0:T(8,128)(2,1)} %param.24) | copy-start | bytes 1572868
  48.2 2.5 %copy-start.15 = (bf16[128,64]{0,1:T(8,128)(2,1)S(1)}, bf16[128,64]{0,1:T(8,128)(2,1)}, u32[]{:S(2)}) copy-start(bf16[128,64]{0,1:T(8,128)(2,1)} %param.25) | copy-start | bytes 49156
  52.4 1.5 %copy-start.12 = (bf16[2048,128]{1,0:T(8,128)(2,1)S(1)}, bf16[2048,128]{1,0:T(8,128)(2,1)}, u32[]{:S(2)}) copy-start(bf16[2048,128]{1,0:T(8,128)(2,1)} %param.26) | copy-start | bytes 1572868
  52.4 1.5 %copy-start.16 = (bf16[128,64]{0,1:T(8,128)(2,1)S(1)}, bf16[128,64]{0,1:T(8,128)(2,1)}, u32[]{:S(2)}) copy-start(bf16[128,64]{0,1:T(8,128)(2,1)} %param.27) | copy-start | bytes 49156
  81.0 0.9 copy-start.13
  83.1 1.1 copy-start.3
  83.1 1.1 copy-start.5
  83.1 1.1 copy-start.7
  84.1 0.8 copy-start.1
  87.1 2.5 %copy-start.2 = (bf16[2,16,64,128]{3,2,1,0:T(8,128)(2,1)S(1)}, bf16[2,16,64,128]{3,2,1,0:T(8,128)(2,1)}, u32[]{:S(2)}) copy-start(bf16[2,16,64,128]{3,2,1,0:T(8,128)(2,1)} %copy-done.1) | copy-start | bytes 1572868 | tf_op jit(solution)/shard_map/while
  89.6 2.2 %copy-start.17 = (s32[4]{0:T(128)S(1)}, s32[4]{0:T(128)}, u32[]{:S(2)}) copy-start(s32[4]{0:T(128)} %get-tuple-element.302) | copy-start | bytes 52 | tf_op jit(solution)/shard_map/while
  90.5 3.6 %copy-start.4 = (bf16[16,64,2,128]{3,1,0,2:T(8,128)(2,1)S(1)}, bf16[16,64,2,128]{3,1,0,2:T(8,128)(2,1)}, u32[]{:S(2)}) copy-start(bf16[16,64,2,128]{3,1,0,2:T(8,128)(2,1)} %copy-done.3) | copy-start | bytes 1572868 | tf_op jit(solution)/shard_map/while
  90.5 3.6 %copy-start.6 = (bf16[4,64,8,64]{1,3,2,0:T(8,128)(2,1)S(1)}, bf16[4,64,8,64]{1,3,2,0:T(8,128)(2,1)}, u32[]{:S(2)}) copy-start(bf16[4,64,8,64]{1,3,2,0:T(8,128)(2,1)} %copy-done.5) | copy-start | bytes 786436 | tf_op jit(solution)/shard_map/while
  90.5 3.6 %copy-start.8 = (bf16[4,64,2,128]{3,1,2,0:T(8,128)(2,1)S(1)}, bf16[4,64,2,128]{3,1,2,0:T(8,128)(2,1)}, u32[]{:S(2)}) copy-start(bf16[4,64,2,128]{3,1,2,0:T(8,128)(2,1)} %copy-done.7) | copy-start | bytes 393220 | tf_op jit(solution)/shard_map/while
  94.1 1.1 copy-start.3
  94.1 1.1 copy-start.5
  94.1 1.1 copy-start.7
  95.1 0.8 copy-start.1
  98.0 2.5 %copy-start.2 = (bf16[2,16,64,128]{3,2,1,0:T(8,128)(2,1)S(1)}, bf16[2,16,64,128]{3,2,1,0:T(8,128)(2,1)}, u32[]{:S(2)}) copy-start(bf16[2,16,64,128]{3,2,1,0:T(8,128)(2,1)} %copy-done.1) | copy-start | bytes 1572868 | tf_op jit(solution)/shard_map/while
  100.6 2.2 %copy-start.17 = (s32[4]{0:T(128)S(1)}, s32[4]{0:T(128)}, u32[]{:S(2)}) copy-start(s32[4]{0:T(128)} %get-tuple-element.302) | copy-start | bytes 52 | tf_op jit(solution)/shard_map/while
  101.5 3.6 %copy-start.4 = (bf16[16,64,2,128]{3,1,0,2:T(8,128)(2,1)S(1)}, bf16[16,64,2,128]{3,1,0,2:T(8,128)(2,1)}, u32[]{:S(2)}) copy-start(bf16[16,64,2,128]{3,1,0,2:T(8,128)(2,1)} %copy-done.3) | copy-start | bytes 1572868 | tf_op jit(solution)/shard_map/while
  101.5 3.6 %copy-start.6 = (bf16[4,64,8,64]{1,3,2,0:T(8,128)(2,1)S(1)}, bf16[4,64,8,64]{1,3,2,0:T(8,128)(2,1)}, u32[]{:S(2)}) copy-start(bf16[4,64,8,64]{1,3,2,0:T(8,128)(2,1)} %copy-done.5) | copy-start | bytes 786436 | tf_op jit(solution)/shard_map/while
  101.5 3.6 %copy-start.8 = (bf16[4,64,2,128]{3,1,2,0:T(8,128)(2,1)S(1)}, bf16[4,64,2,128]{3,1,2,0:T(8,128)(2,1)}, u32[]{:S(2)}) copy-start(bf16[4,64,2,128]{3,1,2,0:T(8,128)(2,1)} %copy-done.7) | copy-start | bytes 393220 | tf_op jit(solution)/shard_map/while
  105.1 1.1 copy-start.3
  105.1 1.1 copy-start.5
  105.1 1.1 copy-start.7
  106.1 0.8 copy-start.1
  109.0 2.5 %copy-start.2 = (bf16[2,16,64,128]{3,2,1,0:T(8,128)(2,1)S(1)}, bf16[2,16,64,128]{3,2,1,0:T(8,128)(2,1)}, u32[]{:S(2)}) copy-start(bf16[2,16,64,128]{3,2,1,0:T(8,128)(2,1)} %copy-done.1) | copy-start | bytes 1572868 | tf_op jit(solution)/shard_map/while
  111.5 2.2 %copy-start.17 = (s32[4]{0:T(128)S(1)}, s32[4]{0:T(128)}, u32[]{:S(2)}) copy-start(s32[4]{0:T(128)} %get-tuple-element.302) | copy-start | bytes 52 | tf_op jit(solution)/shard_map/while
  112.5 3.6 %copy-start.4 = (bf16[16,64,2,128]{3,1,0,2:T(8,128)(2,1)S(1)}, bf16[16,64,2,128]{3,1,0,2:T(8,128)(2,1)}, u32[]{:S(2)}) copy-start(bf16[16,64,2,128]{3,1,0,2:T(8,128)(2,1)} %copy-done.3) | copy-start | bytes 1572868 | tf_op jit(solution)/shard_map/while
  112.5 3.6 %copy-start.6 = (bf16[4,64,8,64]{1,3,2,0:T(8,128)(2,1)S(1)}, bf16[4,64,8,64]{1,3,2,0:T(8,128)(2,1)}, u32[]{:S(2)}) copy-start(bf16[4,64,8,64]{1,3,2,0:T(8,128)(2,1)} %copy-done.5) | copy-start | bytes 786436 | tf_op jit(solution)/shard_map/while
  112.5 3.6 %copy-start.8 = (bf16[4,64,2,128]{3,1,2,0:T(8,128)(2,1)S(1)}, bf16[4,64,2,128]{3,1,2,0:T(8,128)(2,1)}, u32[]{:S(2)}) copy-start(bf16[4,64,2,128]{3,1,2,0:T(8,128)(2,1)} %copy-done.7) | copy-start | bytes 393220 | tf_op jit(solution)/shard_map/while
  116.0 1.1 copy-start.3
  116.1 1.1 copy-start.5
  116.1 1.1 copy-start.7
  117.1 0.8 copy-start.1
  120.0 2.5 %copy-start.2 = (bf16[2,16,64,128]{3,2,1,0:T(8,128)(2,1)S(1)}, bf16[2,16,64,128]{3,2,1,0:T(8,128)(2,1)}, u32[]{:S(2)}) copy-start(bf16[2,16,64,128]{3,2,1,0:T(8,128)(2,1)} %copy-done.1) | copy-start | bytes 1572868 | tf_op jit(solution)/shard_map/while
  122.5 2.2 %copy-start.17 = (s32[4]{0:T(128)S(1)}, s32[4]{0:T(128)}, u32[]{:S(2)}) copy-start(s32[4]{0:T(128)} %get-tuple-element.302) | copy-start | bytes 52 | tf_op jit(solution)/shard_map/while
  123.5 3.6 %copy-start.4 = (bf16[16,64,2,128]{3,1,0,2:T(8,128)(2,1)S(1)}, bf16[16,64,2,128]{3,1,0,2:T(8,128)(2,1)}, u32[]{:S(2)}) copy-start(bf16[16,64,2,128]{3,1,0,2:T(8,128)(2,1)} %copy-done.3) | copy-start | bytes 1572868 | tf_op jit(solution)/shard_map/while
  123.5 3.6 %copy-start.6 = (bf16[4,64,8,64]{1,3,2,0:T(8,128)(2,1)S(1)}, bf16[4,64,8,64]{1,3,2,0:T(8,128)(2,1)}, u32[]{:S(2)}) copy-start(bf16[4,64,8,64]{1,3,2,0:T(8,128)(2,1)} %copy-done.5) | copy-start | bytes 786436 | tf_op jit(solution)/shard_map/while
  123.5 3.6 %copy-start.8 = (bf16[4,64,2,128]{3,1,2,0:T(8,128)(2,1)S(1)}, bf16[4,64,2,128]{3,1,2,0:T(8,128)(2,1)}, u32[]{:S(2)}) copy-start(bf16[4,64,2,128]{3,1,2,0:T(8,128)(2,1)} %copy-done.7) | copy-start | bytes 393220 | tf_op jit(solution)/shard_map/while
where the time goes:
time: 141 us; the launch traced here: 140 us
  blocking collectives  70.7 us (50%)
  local copies, waits for them, and re-layouts  33.9 us (24%)
  matrix products  18.3 us (13%)
  other arithmetic  15.8 us (11%)
    all_gather x1, blocking collectives, shards(): every_list = lax.all_gather(picks[None, :, :, 1:], 'kv', axis=0, tiled=True)  23.3 us
    all_gather x1, blocking collectives, shards(): lax.all_gather(cmp_piece, 'kv', axis=1, tiled=True)  19.1 us
    all_gather x1, blocking collectives, shards(): lax.all_gather(export, 'kv', axis=0, tiled=True)  18.9 us
    all_gather x1, blocking collectives, shards(): lax.all_gather(mixed, 'tp', axis=1, tiled=True).astype(jnp.float32)  9.43 us
    dynamic_slice x16, local copies, waits for them, and re-layouts, shards(): lax.map(one_sequence, (queries, remote_entries, picks, sel_pairs, gates,...  8.72 us
    unnamed x24, local copies, waits for them, and re-layouts  8.52 us
    sub x8, other arithmetic, masked_weights(): expd = jnp.where(valid, jnp.exp(scores - top), 0.0)  7.55 us
    dot_general x5, matrix products, project(): jnp.dot(rows, weight_matrix, preferred_element_type=jnp.float32)  6.41 us

commit v1 on v0

--- a/solution.py
+++ b/solution.py
@@ -1,6 +1,10 @@
+import functools
+
 import jax
 import jax.numpy as jnp
 from jax import lax
+from jax.experimental import pallas as pl
+from jax.experimental.pallas import tpu as pltpu
 from jax.sharding import PartitionSpec as P
 
 HEADS = 16
@@ -182,6 +186,518 @@
     return (total * row_scale[:, None]).astype(jnp.bfloat16).reshape(seqs, span, out_width)
 
 
+FAR = -1e30
+PLANE = 4
+BLOB_EXTRA = 2
+VMEM_BYTES = 60 * 1024 * 1024
+f32 = jnp.float32
+bf16 = jnp.bfloat16
+
+
+def dot(a, b):
+    return jnp.dot(a, b, preferred_element_type=f32)
+
+
+def dot_t(a, b):
+    return lax.dot_general(a, b, (((1,), (1,)), ((), ())), preferred_element_type=f32)
+
+
+def turn(values, cosine, sine):
+    lane = lax.broadcasted_iota(jnp.int32, values.shape, 1)
+    other = jnp.where(
+        lane % HEAD_DIM < HEAD_DIM // 2,
+        pltpu.roll(values, 128 - HEAD_DIM // 2, 1),
+        pltpu.roll(values, HEAD_DIM // 2, 1),
+    )
+    return values * cosine + other * sine
+
+
+def gelu(x):
+    return 0.5 * x * (1.0 + jnp.tanh(0.7978845608028654 * (x + 0.044715 * (x * x * x))))
+
+
+def project_kernel(
+    seqs, span, steps,
+    rows_ref, wq_ref, wck_ref, wcv_ref, wsk_ref, wsv_ref, wg_ref, tables_ref, cout_ref,
+    ckin_ref, cvin_ref,
+    q_ref, sk_ref, sv_ref, ck_ref, cv_ref, gate_ref,
+    acc_q, acc_p, acc_g, raw, kin, vin, sems,
+):
+    step = pl.program_id(0)
+    load_k = pltpu.make_async_copy(ckin_ref, kin, sems.at[0])
+    load_v = pltpu.make_async_copy(cvin_ref, vin, sems.at[1])
+
+    @pl.when(step == 0)
+    def _():
+        load_k.start()
+        load_v.start()
+        acc_q[...] = jnp.zeros_like(acc_q)
+        acc_p[...] = jnp.zeros_like(acc_p)
+        acc_g[...] = jnp.zeros_like(acc_g)
+
+    rows = rows_ref[...]
+    acc_q[...] += dot(rows, wq_ref[...])
+    for i, ref in enumerate((wck_ref, wcv_ref, wsk_ref, wsv_ref)):
+        acc_p[i] += dot(rows, ref[...])
+    acc_g[...] += dot(rows, wg_ref[...])
+
+    @pl.when(step == steps - 1)
+    def _():
+        count = span // CMP_STRIDE
+        entries = seqs * count
+        cosine = tables_ref[0, :span]
+        sine = tables_ref[1, :span]
+        heads = acc_q.shape[1] // HEAD_DIM
+        lane = lax.broadcasted_iota(jnp.int32, (span, 128), 1)
+        low = lane < HEAD_DIM
+        gate_ref[...] = jax.nn.sigmoid(acc_g[...])
+        for s in range(seqs):
+            part = pl.ds(s * span, span)
+            sk_ref[part, :] = turn(acc_p[2, part, :], cosine, sine).astype(bf16)
+            for i in range(heads // 2):
+                x = turn(acc_q[part, i * 128 : (i + 1) * 128], cosine, sine)
+                x = x * (HEAD_DIM**-0.5)
+                y = pltpu.roll(x, HEAD_DIM, 1)
+                if 2 * i < heads // 2:
+                    even, odd = jnp.where(low, x, 0.0), jnp.where(low, y, 0.0)
+                else:
+                    even, odd = jnp.where(low, 0.0, y), jnp.where(low, 0.0, x)
+                base = (s * heads + 2 * i) * span
+                q_ref[base : base + span, :] = even.astype(bf16)
+                q_ref[base + span : base + 2 * span, :] = odd.astype(bf16)
+        sv_ref[...] = acc_p[3].astype(bf16)
+        raw[...] = acc_p[0:2].astype(bf16).astype(f32)
+        low_e = lax.broadcasted_iota(jnp.int32, (entries, 128), 1) < HEAD_DIM
+        first = lax.broadcasted_iota(jnp.int32, (entries, 128), 0) % count == 0
+        load_k.wait()
+        load_v.wait()
+        half = CMP_STRIDE * HEAD_DIM
+        for branch, weight, out_ref in ((0, kin, ck_ref), (1, vin, cv_ref)):
+            left, right = [], []
+            for j in range(0, CMP_STRIDE, 2):
+                a = raw[branch, pl.ds(j, entries, stride=CMP_STRIDE), :]
+                b = raw[branch, pl.ds(j + 1, entries, stride=CMP_STRIDE), :]
+                left.append(jnp.where(low_e, a, pltpu.roll(b, HEAD_DIM, 1)))
+                right.append(jnp.where(low_e, pltpu.roll(a, HEAD_DIM, 1), b))
+            window = jnp.concatenate(
+                [jnp.concatenate(left, axis=1), jnp.concatenate(right, axis=1)], axis=0
+            ).astype(bf16)
+            front = dot(window, weight[:half])
+            back = dot(window, weight[half:])
+            parts = []
+            for g in range(2):
+                shifted = pltpu.roll(front[g * entries : (g + 1) * entries], 1, 0)
+                parts.append(back[g * entries : (g + 1) * entries] + jnp.where(first, 0.0, shifted))
+            inner = gelu(jnp.concatenate(parts, axis=0)).astype(bf16)
+            made = dot(inner, cout_ref[branch])
+            made = jnp.where(low_e, made[:entries], made[entries:])
+            if branch == 0:
+                made = turn(made, tables_ref[0, span:], tables_ref[1, span:])
+            out_ref[...] = made.astype(bf16)
+
+
+def gather_kernel(
+    n, seqs, span,
+    picks_ref, sk_ref, sv_ref, ck_ref, cv_ref,
+    all_ref,
+    lists, pick_send, pick_recv, send, recv,
+):
+    me = lax.axis_index("kv")
+    planes = n // PLANE
+    z, x, c = me // PLANE, (me // 2) % 2, me % 2
+    barrier = pltpu.get_barrier_semaphore()
+    for d in range(1, n):
+        pl.semaphore_signal(
+            barrier, inc=1, device_id={"kv": (me + d) % n},
+            device_id_type=pl.DeviceIdType.MESH,
+        )
+    pl.semaphore_wait(barrier, n - 1)
+
+    sent = []
+    for d in range(1, n):
+        copy = pltpu.make_async_remote_copy(
+            src_ref=picks_ref, dst_ref=lists.at[me], send_sem=pick_send.at[d - 1],
+            recv_sem=pick_recv.at[me], device_id={"kv": (me + d) % n},
+            device_id_type=pl.DeviceIdType.MESH,
+        )
+        copy.start()
+        sent.append(copy)
+
+    entries = ck_ref.shape[0]
+    all_ref[me, 2 * span : 2 * span + entries, :] = ck_ref[...]
+    all_ref[me, 2 * span + entries :, :] = cv_ref[...]
+
+    named = jnp.zeros((1, 128), jnp.int32)
+    for d in range(1, n):
+        origin = (me + d) % n
+        pltpu.make_async_remote_copy(
+            src_ref=picks_ref, dst_ref=lists.at[origin], send_sem=pick_send.at[d - 1],
+            recv_sem=pick_recv.at[origin], device_id={"kv": origin},
+            device_id_type=pl.DeviceIdType.MESH,
+        ).wait_recv()
+        named = jnp.maximum(named, (lists[origin] == me).astype(jnp.int32))
+    at = lax.broadcasted_iota(jnp.int32, (1, 128), 1)
+    low = at < HEAD_DIM
+    named = jnp.where(at % TOPK == 0, 0, named)
+    key = jnp.zeros((span, 128), f32)
+    value = jnp.zeros((span, 128), f32)
+    for s in range(seqs):
+        flags = [
+            jnp.max(jnp.where(at // TOPK == s * 2 + g, named, 0), axis=1, keepdims=True)
+            for g in range(2)
+        ]
+        flag = jnp.where(low, flags[0], flags[1]) > 0
+        key = jnp.where(flag, sk_ref[s * span : (s + 1) * span, :].astype(f32), key)
+        value = jnp.where(flag, sv_ref[s * span : (s + 1) * span, :].astype(f32), value)
+    all_ref[me, 0:span, :] = key.astype(bf16)
+    all_ref[me, span : 2 * span, :] = value.astype(bf16)
+
+    def pass_on(slot, dst, number):
+        copy = pltpu.make_async_remote_copy(
+            src_ref=all_ref.at[slot], dst_ref=all_ref.at[slot], send_sem=send.at[number],
+            recv_sem=recv.at[slot], device_id={"kv": dst},
+            device_id_type=pl.DeviceIdType.MESH,
+        )
+        copy.start()
+        sent.append(copy)
+
+    def arrived(slot):
+        pltpu.make_async_remote_copy(
+            src_ref=all_ref.at[slot], dst_ref=all_ref.at[slot], send_sem=send.at[0],
+            recv_sem=recv.at[slot], device_id={"kv": (me + 1) % n},
+            device_id_type=pl.DeviceIdType.MESH,
+        ).wait_recv()
+
+    across = z * PLANE + (1 - x) * 2 + c
+    beside = z * PLANE + x * 2 + (1 - c)
+    number = 0
+    for d in range(1, planes):
+        pass_on(me, ((z + d) % planes) * PLANE + x * 2 + c, number)
+        number += 1
+    pass_on(me, across, number)
+    pass_on(me, beside, number + 1)
+    number += 2
+    order = [0] + [d for d in range(1, planes)]
+    for d in order:
+        origin = ((z + planes - d) % planes) * PLANE
+        if d > 0:
+            slot = origin + x * 2 + c
+            arrived(slot)
+            pass_on(slot, across, number)
+            pass_on(slot, beside, number + 1)
+            number += 2
+    for d in order:
+        origin = ((z + planes - d) % planes) * PLANE
+        slot = origin + (1 - x) * 2 + c
+        arrived(slot)
+        pass_on(slot, beside, number)
+        number += 1
+    for d in order:
+        origin = ((z + planes - d) % planes) * PLANE
+        arrived(origin + x * 2 + (1 - c))
+        arrived(origin + (1 - x) * 2 + (1 - c))
+    for copy in sent:
+        copy.wait_send()
+
+
+def attend_kernel(
+    n, seqs, span, heads,
+    lens_ref, q_ref, sk_ref, sv_ref, all_ref, picks_ref, gate_ref, gain_ref, wout_ref,
+    out_ref,
+    weight, own, other, bias, near, wsem, send, recv,
+):
+    place = lax.axis_index("kv")
+    column = lax.axis_index("tp")
+    depth = heads * HEAD_DIM
+    wide = out_ref.shape[1]
+    loads = []
+    for i in range(2):
+        side = column if i == 0 else 1 - column
+        load = pltpu.make_async_copy(
+            wout_ref.at[
+                pl.ds(pl.multiple_of(side * depth, depth), depth),
+                pl.ds(pl.multiple_of(column * wide, wide), wide),
+            ],
+            weight.at[i],
+            wsem.at[i],
+        )
+        load.start()
+        loads.append(load)
+    barrier = pltpu.get_barrier_semaphore()
+    pl.semaphore_signal(
+        barrier, inc=1, device_id={"tp": 1 - column}, device_id_type=pl.DeviceIdType.MESH
+    )
+
+    count = span // CMP_STRIDE
+    entries = seqs * count
+    far_keys = n * span
+    block = lax.broadcasted_iota(jnp.int32, (seqs * 2, far_keys), 1) // span
+    hit = jnp.zeros((seqs * 2, far_keys), jnp.int32)
+    lists = picks_ref[...]
+    for j in range(1, TOPK):
+        hit = jnp.where(block == lists[:, j : j + 1], 1, hit)
+    bias[...] = jnp.where(hit > 0, 0.0, FAR)
+    row_q = lax.broadcasted_iota(jnp.int32, (span, span), 0)
+    near[...] = jnp.where(
+        lax.broadcasted_iota(jnp.int32, (span, span), 1) <= row_q, 0.0, FAR
+    )
+    slot = lax.broadcasted_iota(jnp.int32, (span, n * entries), 1)
+    entry = (slot // entries) * count + slot % count
+    entry_seq = (slot % entries) // count
+    at = place * span + lax.broadcasted_iota(jnp.int32, (span, n * entries), 0)
+    entry_ok = (entry >= 1) & (entry * CMP_STRIDE + CMP_STRIDE - 1 <= at)
+    low = lax.broadcasted_iota(jnp.int32, (span, 128), 1) < HEAD_DIM
+    row_at = place * span + lax.broadcasted_iota(jnp.int32, (span, 128), 0)
+    far_k = all_ref[:, 0:span, :].reshape(far_keys, 128)
+    far_v = all_ref[:, span : 2 * span, :].reshape(far_keys, 128)
+    cmp_k = all_ref[:, 2 * span : 2 * span + entries, :].reshape(n * entries, 128)
+    cmp_v = all_ref[:, 2 * span + entries :, :].reshape(n * entries, 128)
+    pl.semaphore_wait(barrier, 1)
+
+    def piece(s):
+        return pltpu.make_async_remote_copy(
+            src_ref=own.at[s], dst_ref=other.at[s], send_sem=send.at[s], recv_sem=recv.at[s],
+            device_id={"tp": 1 - column}, device_id_type=pl.DeviceIdType.MESH,
+        )
+
+    half = heads // 2
+
+    def one_sequence(s, carry):
+        rows = pl.ds(pl.multiple_of(s * span, span), span)
+        near_k = sk_ref[rows, :]
+        near_v = sv_ref[rows, :]
+        gates = gate_ref[rows, :]
+        length = lens_ref[s]
+        live = row_at < length
+        entry_bias = jnp.where(entry_ok & (entry_seq == s), 0.0, FAR)
+        for g in range(2):
+            start = pl.multiple_of((s * heads + g * half) * span, span)
+            q = q_ref[pl.ds(start, half * span), :]
+            sc = dot_t(q, cmp_k).reshape(half, span, n * entries) + entry_bias[None]
+            top = jnp.maximum(jnp.max(sc, axis=-1, keepdims=True), -1e29)
+            e = jnp.exp(sc - top)
+            total = jnp.maximum(jnp.sum(e, axis=-1, keepdims=True), 1.0)
+            w = (e * (1.0 / total)).astype(bf16).reshape(half * span, n * entries)
+            cmp_out = dot(w, cmp_v)
+            sf = dot_t(q, far_k) + bias[pl.ds(s * 2 + g, 1), :]
+            sn = (dot_t(q, near_k).reshape(half, span, span) + near[...][None]).reshape(
+                half * span, span
+            )
+            top = jnp.maximum(
+                jnp.max(sf, axis=-1, keepdims=True), jnp.max(sn, axis=-1, keepdims=True)
+            )
+            ef = jnp.exp(sf - top)
+            en = jnp.exp(sn - top)
+            total = jnp.sum(ef, axis=-1, keepdims=True) + jnp.sum(en, axis=-1, keepdims=True)
+            inverse = 1.0 / total
+            sel_out = dot((ef * inverse).astype(bf16), far_v) + dot(
+                (en * inverse).astype(bf16), near_v
+            )
+            mixed = []
+            for h in range(half):
+                part = slice(h * span, (h + 1) * span)
+                head = g * half + h
+                mixed.append(
+                    gates[:, head : head + 1] * cmp_out[part]
+                    + gates[:, heads + head : heads + head + 1] * sel_out[part]
+                )
+            for h in range(0, half, 2):
+                if g == 0:
+                    pair = jnp.where(low, mixed[h], pltpu.roll(mixed[h + 1], HEAD_DIM, 1))
+                else:
+                    pair = jnp.where(low, pltpu.roll(mixed[h], HEAD_DIM, 1), mixed[h + 1])
+                pair = jnp.where(live, pair, 0.0).astype(bf16)
+                lanes = (g * half + h) * HEAD_DIM
+                own[s, :, lanes : lanes + 128] = pair
+        piece(s).start()
+        return carry
+
+    lax.fori_loop(0, seqs, one_sequence, 0)
+    for load in loads:
+        load.wait()
+    gain_own = gain_ref[pl.ds(column, 1), :]
+    gain_other = gain_ref[pl.ds(1 - column, 1), :]
+
+    def finish(s, carry):
+        piece(s).wait_recv()
+        a = own[s].astype(f32)
+        b = other[s].astype(f32)
+        squares = jnp.sum(a * a, axis=-1, keepdims=True) + jnp.sum(b * b, axis=-1, keepdims=True)
+        row_scale = lax.rsqrt(squares / (2 * depth) + norm_eps)
+        total = dot((a * gain_own).astype(bf16), weight[0]) + dot(
+            (b * gain_other).astype(bf16), weight[1]
+        )
+        out_ref[pl.ds(pl.multiple_of(s * span, span), span), :] = (total * row_scale).astype(bf16)
+        return carry
+
+    lax.fori_loop(0, seqs, finish, 0)
+
+    def close(s, carry):
+        piece(s).wait_send()
+        return carry
+
+    lax.fori_loop(0, seqs, close, 0)
+
+
+def fused_shards(
+    hidden_in,
+    w_query,
+    w_cmp_key,
+    w_cmp_value,
+    w_sel_key,
+    w_sel_value,
+    w_gate,
+    cmp_key_in,
+    cmp_key_out,
+    cmp_value_in,
+    cmp_value_out,
+    out_gain,
+    w_out,
+    seq_lengths,
+    chosen,
+):
+    seqs, span, width = hidden_in.shape
+    n = lax.axis_size("kv")
+    place = lax.axis_index("kv")
+    column = lax.axis_index("tp")
+    heads = w_query.shape[1] // HEAD_DIM
+    count = span // CMP_STRIDE
+    entries = seqs * count
+    total = seqs * span
+    out_width = width // lax.axis_size("tp")
+    vmem = pl.BlockSpec(memory_space=pltpu.VMEM)
+    anywhere = pl.BlockSpec(memory_space=pl.ANY)
+
+    rows = hidden_in.reshape(total, width)
+    gate_weight = lax.dynamic_slice_in_dim(w_gate, column * heads, heads, 2).reshape(
+        width, 2 * heads
+    )
+    positions = place * span + jnp.concatenate(
+        [
+            jnp.arange(span, dtype=jnp.int32),
+            jnp.tile(jnp.arange(count, dtype=jnp.int32) * CMP_STRIDE + CMP_STRIDE - 1, seqs),
+        ]
+    )
+    lane = jnp.arange(128, dtype=jnp.int32)
+    power = (lane % (HEAD_DIM // 2) * 2).astype(f32)
+    inverse = jnp.exp(-jnp.log(f32(theta_base)) * power / HEAD_DIM)
+    angle = positions.astype(f32)[:, None] * inverse[None, :]
+    sign = jnp.where(lane % HEAD_DIM < HEAD_DIM // 2, -1.0, 1.0)
+    tables = jnp.stack([jnp.cos(angle), jnp.sin(angle) * sign[None, :]])
+    second = jnp.stack(
+        [
+            jnp.concatenate([cmp_key_out, cmp_key_out], axis=1),
+            jnp.concatenate([cmp_value_out, cmp_value_out], axis=1),
+        ]
+    )
+
+    steps = 4
+    depth = width // steps
+
+    def by_depth(weight_matrix):
+        return pl.BlockSpec((depth, weight_matrix.shape[1]), lambda k: (k, 0))
+
+    def whole(*shape):
+        return pl.BlockSpec(shape, lambda k: (0,) * len(shape))
+
+    small = w_sel_key.shape[1]
+    q, sk, sv, ck, cv, gates = pl.pallas_call(
+        functools.partial(project_kernel, seqs, span, steps),
+        grid=(steps,),
+        in_specs=[
+            pl.BlockSpec((total, depth), lambda k: (0, k)),
+            by_depth(w_query),
+            by_depth(w_cmp_key),
+            by_depth(w_cmp_value),
+            by_depth(w_sel_key),
+            by_depth(w_sel_value),
+            by_depth(gate_weight),
+            whole(*tables.shape),
+            whole(*second.shape),
+            anywhere,
+            anywhere,
+        ],
+        out_specs=[
+            whole(heads * total, 128),
+            whole(total, small),
+            whole(total, small),
+            whole(entries, small),
+            whole(entries, small),
+            whole(total, 2 * heads),
+        ],
+        out_shape=[
+            jax.ShapeDtypeStruct((heads * total, 128), bf16),
+            jax.ShapeDtypeStruct((total, small), bf16),
+            jax.ShapeDtypeStruct((total, small), bf16),
+            jax.ShapeDtypeStruct((entries, small), bf16),
+            jax.ShapeDtypeStruct((entries, small), bf16),
+            jax.ShapeDtypeStruct((total, 2 * heads), f32),
+        ],
+        scratch_shapes=[
+            pltpu.VMEM((total, heads * HEAD_DIM), f32),
+            pltpu.VMEM((4, total, small), f32),
+            pltpu.VMEM((total, 2 * heads), f32),
+            pltpu.VMEM((2, total, small), f32),
+            pltpu.VMEM(cmp_key_in.shape, bf16),
+            pltpu.VMEM(cmp_value_in.shape, bf16),
+            pltpu.SemaphoreType.DMA((2,)),
+        ],
+        compiler_params=pltpu.CompilerParams(dimension_semantics=("arbitrary",)),
+        name="project",
+    )(
+        rows, w_query, w_cmp_key, w_cmp_value, w_sel_key, w_sel_value, gate_weight,
+        tables, second, cmp_key_in, cmp_value_in,
+    )
+
+    picks = chosen[:, 0]
+    blob = 2 * span + 2 * entries
+    everything = pl.pallas_call(
+        functools.partial(gather_kernel, n, seqs, span),
+        in_specs=[vmem] * 5,
+        out_specs=vmem,
+        out_shape=jax.ShapeDtypeStruct((n, blob, small), bf16),
+        scratch_shapes=[
+            pltpu.VMEM((n, 1, 128), jnp.int32),
+            pltpu.SemaphoreType.DMA((n,)),
+            pltpu.SemaphoreType.DMA((n,)),
+            pltpu.SemaphoreType.DMA((n,)),
+            pltpu.SemaphoreType.DMA((n,)),
+        ],
+        compiler_params=pltpu.CompilerParams(collective_id=0, has_side_effects=True),
+        name="gather",
+    )(picks.reshape(1, 128), sk, sv, ck, cv)
+
+    out = pl.pallas_call(
+        functools.partial(attend_kernel, n, seqs, span, heads),
+        in_specs=[pl.BlockSpec(memory_space=pltpu.SMEM)] + [vmem] * 7 + [anywhere],
+        out_specs=vmem,
+        out_shape=jax.ShapeDtypeStruct((total, out_width), bf16),
+        scratch_shapes=[
+            pltpu.VMEM((2, heads * HEAD_DIM, out_width), bf16),
+            pltpu.VMEM((seqs, span, heads * HEAD_DIM), bf16),
+            pltpu.VMEM((seqs, span, heads * HEAD_DIM), bf16),
+            pltpu.VMEM((seqs * 2, n * span), f32),
+            pltpu.VMEM((span, span), f32),
+            pltpu.SemaphoreType.DMA((2,)),
+            pltpu.SemaphoreType.DMA((seqs,)),
+            pltpu.SemaphoreType.DMA((seqs,)),
+        ],
+        compiler_params=pltpu.CompilerParams(
+            collective_id=1, has_side_effects=True, vmem_limit_bytes=VMEM_BYTES
+        ),
+        name="attend",
+    )(
+        seq_lengths, q, sk, sv, everything, picks.reshape(seqs * 2, TOPK), gates,
+        out_gain.reshape(2, heads * HEAD_DIM), w_out,
+    )
+    return out.reshape(seqs, span, out_width)
+
+
+def fits(mesh):
+    n = mesh.shape["kv"]
+    return mesh.shape["tp"] == 2 and n % PLANE == 0 and n <= 32
+
+
 def solution(mesh):
     placed = (
         P(None, "kv", None),
@@ -201,5 +717,5 @@
         P(None, "kv", "tp", None),
     )
     return jax.shard_map(
-        shards, mesh=mesh, in_specs=placed, out_specs=P(None, "kv", "tp"), check_vma=False
-    )
+        fused_shards if fits(mesh) else shards, mesh=mesh, in_specs=placed, out_specs=P(None, "kv", "tp"), check_vma=False
+    )

time: 141 us -> 55.9 us (0.40)
  blocking collectives: 70.7 us -> 0 us
  Pallas kernels: 0 us -> 46.5 us
  local copies, waits for them, and re-layouts: 33.9 us -> 7.24 us
  matrix products: 18.3 us -> 0 us
  other arithmetic: 15.8 us -> 1.68 us
    all_gather x4 -> x0, blocking collectives: 70.7 us -> none  [the longest x1 23.3 us: shards(): every_list = lax.all_gather(picks[None, :, :, 1:], 'kv', axis=0, tiled=True)]
    pallas_call x0 -> x3, Pallas kernels: none -> 46.5 us  [the longest x1 21.6 us: fused_shards(): pl.pallas_call(functools.partial(gather_kernel, n, seqs, span), in_specs=...]
    dot_general x25 -> x0, matrix products: 18.3 us -> none  [the longest x5 6.41 us: project(): jnp.dot(rows, weight_matrix, preferred_element_type=jnp.float32)]
    dynamic_slice x16 -> x0, local copies, waits for them, and re-layouts: 8.72 us -> none  [shards(): lax.map(one_sequence, (queries, remote_entries, picks, sel_pairs, gates,...]
    sub x9 -> x1, other arithmetic: 7.56 us -> 0.01 us  [fused_shards(): jnp.arange(count, dtype=jnp.int32) * CMP_STRIDE + CMP_STRIDE - 1]
    broadcast_in_dim x16 -> x0, local copies, waits for them, and re-layouts: 5.05 us -> none  [the longest x4 4.28 us: masked_weights(): expd = jnp.where(valid, jnp.exp(scores - top), 0.0)]
    unnamed x24 -> x5, local copies, waits for them, and re-layouts: 8.52 us -> 3.53 us
    gather x8 -> x0, local copies, waits for them, and re-layouts: 3.25 us -> none  [one_sequence(): table[index]]
where the time goes in v1:
time: 55.9 us; the launch traced here: 55.4 us
  Pallas kernels  46.5 us (83%)
  local copies, waits for them, and re-layouts  7.24 us (13%)
  other arithmetic  1.68 us (3%)
    pallas_call x1, Pallas kernels, fused_shards(): pl.pallas_call(functools.partial(gather_kernel, n, seqs, span), in_specs=...  21.6 us
    pallas_call x1, Pallas kernels, fused_shards(): pl.pallas_call(functools.partial(attend_kernel, n, seqs, span, heads), in...  17 us
    pallas_call x1, Pallas kernels, fused_shards(): pl.pallas_call(functools.partial(project_kernel, seqs, span, steps), grid...  7.91 us
    unnamed x5, local copies, waits for them, and re-layouts  3.53 us
    another operation x1, local copies, waits for them, and re-layouts, fused_shards(): picks.reshape(1, 128)  1.34 us
    reshape x1, local copies, waits for them, and re-layouts, fused_shards(): out_gain.reshape(2, heads * HEAD_DIM)  1.28 us

profile of v1, /device:TPU:0, one launch (start us, length us, event | category | flops | bytes accessed | tf_op | source)
XLA Modules:
  0.0 55.4 jit_solution(4470698034229928231)
XLA Ops:
  0.0 0.0 copy-start
  0.0 1.3 %reshape_squeeze.6.picks_ref = s32[1,128]{1,0:T(1,128)} reshape(s32[4,1,2,16]{3,2,1,0:T(2,128)} %param.29) | data formatting | bytes 1024 | tf_op jit(solution)/shard_map/reshape;squeeze | solution.py:668
  1.4 0.1 concatenate.15
  1.4 0.1 fusion.5
  1.5 1.3 %reshape.170.gain_ref = f32[2,512]{1,0:T(2,128)} reshape(f32[1024]{0:T(1024)} %param.26) | data formatting | bytes 8192 | tf_op jit(solution)/shard_map/reshape | solution.py:691
  2.8 0.8 %copy.21 = bf16[128,64]{1,0:T(8,128)(2,1)S(1)} copy(bf16[128,64]{0,1:T(8,128)(2,1)} %param.23) | data formatting | bytes 32768 | tf_op args[8]
  3.6 0.8 %copy.23 = bf16[128,64]{1,0:T(8,128)(2,1)S(1)} copy(bf16[128,64]{0,1:T(8,128)(2,1)} %param.25) | data formatting | bytes 32768 | tf_op args[10]
  4.5 0.1 maximum_bitcast_fusion
  4.6 0.6 %pad_maximum_fusion.1.cout_ref = bf16[2,128,128]{2,1,0:T(8,128)(2,1)} fusion(bf16[1,128,128]{2,1,0:T(8,128)(2,1)S(1)} %get-tuple-element.22, bf16[1,128,128]{2,1,0:T(8,128)(2,1)S(1)} %get-tuple-element.21), kind=kLoop, calls=%fused_computation.1 | loop fusion | flops 32768 | bytes 131072 | tf_op jit(solution)/shard_map/stack | solution.py:587
  5.2 0.0 copy-done
  5.2 0.2 multiply_cosine_fusion
  5.4 0.6 %pad_maximum_fusion.tables_ref = f32[2,80,128]{2,1,0:T(8,128)} fusion(f32[1,80,128]{2,1,0:T(8,128)S(1)} %get-tuple-element.18, f32[1,80,128]{2,1,0:T(8,128)S(1)} %get-tuple-element.17), kind=kLoop, calls=%fused_computation | loop fusion | flops 20480 | bytes 163840 | tf_op jit(solution)/shard_map/stack | solution.py:586
  6.1 1.0 %copy.25.wg_ref = bf16[2048,16]{1,0:T(8,128)(2,1)} copy(bf16[2048,16]{0,1:T(8,128)(2,1)S(1)} %dynamic-slice_bitcast_fusion) | data formatting | bytes 131072 | tf_op jit(solution)/shard_map/reshape | solution.py:572
  7.1 7.9 %project.1 = (bf16[2048,128]{1,0:T(8,128)(2,1)}, bf16[256,128]{1,0:T(8,128)(2,1)}, bf16[256,128]{1,0:T(8,128)(2,1)}, bf16[16,128]{1,0:T(8,128)(2,1)}, bf16[16,128]{1,0:T(8,128)(2,1)}, /*index=5*/f32[256,16]{1,0:T(8,128)}) custom-call(bf16[256,2048]{1,0:T(8,128)(2,1)} %bitcast.10, bf16[2048,512]{1,0:T(8,128)(2,1)} %wq_ref.1, bf16[2048,128]{1,0:T(8,128)(2,1)} %wck_ref.1, ...), custom_call_target="tpu_custom_call" | custom-call | tf_op jit(solution)/shard_map/project/pallas_call | solution.py:604
  15.0 21.6 %gather.1.all_ref = bf16[16,160,128]{2,1,0:T(8,128)(2,1)} custom-call(s32[1,128]{1,0:T(1,128)} %reshape_squeeze.6.picks_ref, bf16[256,128]{1,0:T(8,128)(2,1)} %get-tuple-element.12.sk_ref, bf16[256,128]{1,0:T(8,128)(2,1)} %get-tuple-element.13.sv_ref, bf16[16,128]{1,0:T(8,128)(2,1)} %get-tuple-element.14.ck_ref, bf16[16,128]{1,0:T(8,128)(2,1)} %get-tuple-element.15.cv_ref), custom_call_target="tpu_custom_call" | custom-call | tf_op jit(solution)/shard_map/gather/pallas_call | solution.py:654
  36.6 17.0 %attend.1 = bf16[256,1024]{1,0:T(8,128)(2,1)} custom-call(s32[4]{0:T(128)} %lens_ref.1, bf16[2048,128]{1,0:T(8,128)(2,1)} %get-tuple-element.11.q_ref, bf16[256,128]{1,0:T(8,128)(2,1)} %get-tuple-element.12.sk_ref, bf16[256,128]{1,0:T(8,128)(2,1)} %get-tuple-element.13.sv_ref, bf16[16,160,128]{2,1,0:T(8,128)(2,1)} %gather.1.all_ref, s32[8,16]{1,0:T(8,128)} %bitcast.11, ...), custom_call_target="tpu_custom_call" | custom-call | tf_op jit(solution)/shard_map/attend/pallas_call | solution.py:670
  53.6 1.9 %copy.27 = bf16[4,64,1024]{2,1,0:T(8,128)(2,1)} copy(bf16[4,64,1024]{2,1,0:T(8,128)(2,1)} %bitcast.9) | data formatting | bytes 1048576
  (5 shorter events, 0.0 us)
Async XLA Ops:
  0.0 5.2 %copy-start = (bf16[2048,2,16]{0,2,1:T(8,128)(2,1)S(1)}, bf16[2048,2,16]{0,2,1:T(8,128)(2,1)}, u32[]{:S(2)}) copy-start(bf16[2048,2,16]{0,2,1:T(8,128)(2,1)} %param.21) | copy-start | bytes 393220

commit v2 on v0

--- a/solution.py
+++ b/solution.py
@@ -1,6 +1,10 @@
+import functools
+
 import jax
 import jax.numpy as jnp
 from jax import lax
+from jax.experimental import pallas as pl
+from jax.experimental.pallas import tpu as pltpu
 from jax.sharding import PartitionSpec as P
 
 HEADS = 16
@@ -182,6 +186,404 @@
     return (total * row_scale[:, None]).astype(jnp.bfloat16).reshape(seqs, span, out_width)
 
 
+FAR = -1e30
+PLANE = 4
+VMEM_BYTES = 60 * 1024 * 1024
+f32 = jnp.float32
+bf16 = jnp.bfloat16
+
+
+def dot(a, b):
+    return jnp.dot(a, b, preferred_element_type=f32)
+
+
+def dot_t(a, b):
+    return lax.dot_general(a, b, (((1,), (1,)), ((), ())), preferred_element_type=f32)
+
+
+def turn(values, cosine, sine):
+    lane = lax.broadcasted_iota(jnp.int32, values.shape, 1)
+    other = jnp.where(
+        lane % HEAD_DIM < HEAD_DIM // 2,
+        pltpu.roll(values, 128 - HEAD_DIM // 2, 1),
+        pltpu.roll(values, HEAD_DIM // 2, 1),
+    )
+    return values * cosine + other * sine
+
+
+def gelu(x):
+    return 0.5 * x * (1.0 + jnp.tanh(0.7978845608028654 * (x + 0.044715 * (x * x * x))))
+
+
+def layer_kernel(
+    n, seqs, span, heads,
+    lens_ref, picks_ref, freq_ref, gain_ref, kout_ref, vout_ref,
+    rows_ref, wq_ref, wck_ref, wcv_ref, wsk_ref, wsv_ref, wg_ref, kin_ref, vin_ref, wout_ref,
+    out_ref,
+    rows, wq, ws, wg, kin, vin, weight,
+    q_buf, sk_buf, sv_buf, raw, gate_buf, lists, blobs, own, other, bias, near,
+    load_sem, pick_send, pick_recv, blob_send, blob_recv, half_send, half_recv,
+):
+    me = lax.axis_index("kv")
+    column = lax.axis_index("tp")
+    planes = n // PLANE
+    z, x, c = me // PLANE, (me // 2) % 2, me % 2
+    depth = heads * HEAD_DIM
+    wide = out_ref.shape[1]
+    count = span // CMP_STRIDE
+    entries = seqs * count
+    half = heads // 2
+    mesh_id = pl.DeviceIdType.MESH
+
+    pairs = [(rows_ref, rows)]
+    for i, ref in enumerate((wsk_ref, wsv_ref, wck_ref, wcv_ref)):
+        pairs.append((ref, ws.at[:, i * 128 : (i + 1) * 128]))
+    pairs += [(kin_ref, kin), (vin_ref, vin), (wq_ref, wq), (wg_ref, wg)]
+    for i in range(2):
+        side = column if i == 0 else 1 - column
+        block = wout_ref.at[
+            pl.ds(pl.multiple_of(side * depth, depth), depth),
+            pl.ds(pl.multiple_of(column * wide, wide), wide),
+        ]
+        pairs.append((block, weight.at[i]))
+    loads = [pltpu.make_async_copy(a, b, load_sem.at[i]) for i, (a, b) in enumerate(pairs)]
+    for load in loads:
+        load.start()
+
+    barrier = pltpu.get_barrier_semaphore()
+    for d in range(1, n):
+        pl.semaphore_signal(
+            barrier, inc=1, device_id={"kv": (me + d) % n}, device_id_type=mesh_id
+        )
+    pl.semaphore_signal(barrier, inc=1, device_id={"tp": 1 - column}, device_id_type=mesh_id)
+
+    lane = lax.broadcasted_iota(jnp.int32, (span, 128), 1)
+    low = lane < HEAD_DIM
+    low_e = low[:entries]
+    at = lax.broadcasted_iota(jnp.int32, (span, 128), 0)
+    sign = jnp.where(lane % HEAD_DIM < HEAD_DIM // 2, -1.0, 1.0)
+    angle = (me * span + at).astype(f32) * freq_ref[...]
+    cosine = jnp.cos(angle)
+    sine = jnp.sin(angle) * sign
+    end = me * span + (at[:entries] % count) * CMP_STRIDE + CMP_STRIDE - 1
+    angle = end.astype(f32) * freq_ref[...]
+    cosine_e = jnp.cos(angle)
+    sine_e = jnp.sin(angle) * sign[:entries]
+    row_q = lax.broadcasted_iota(jnp.int32, (span, span), 0)
+    near[...] = jnp.where(
+        lax.broadcasted_iota(jnp.int32, (span, span), 1) <= row_q, 0.0, FAR
+    )
+    far_keys = n * span
+    block = lax.broadcasted_iota(jnp.int32, (2, far_keys), 1) // span
+    for s in range(seqs):
+        listed = picks_ref[s]
+        hit = jnp.zeros((2, far_keys), jnp.int32)
+        for j in range(1, TOPK):
+            hit = jnp.where(block == listed[:, j : j + 1], 1, hit)
+        bias[s] = jnp.where(hit > 0, 0.0, FAR)
+
+    pl.semaphore_wait(barrier, n)
+    sent = []
+    for d in range(1, n):
+        copy = pltpu.make_async_remote_copy(
+            src_ref=picks_ref, dst_ref=lists.at[me], send_sem=pick_send.at[d - 1],
+            recv_sem=pick_recv.at[me], device_id={"kv": (me + d) % n}, device_id_type=mesh_id,
+        )
+        copy.start()
+        sent.append(copy)
+
+    for load in loads[:5]:
+        load.wait()
+    made = dot(rows[...], ws[...])
+    for s in range(seqs):
+        part = slice(s * span, (s + 1) * span)
+        sk_buf[part, :] = turn(made[part, :128], cosine, sine).astype(bf16)
+    sv_buf[...] = made[:, 128:256].astype(bf16)
+    raw[0] = made[:, 256:384].astype(bf16).astype(f32)
+    raw[1] = made[:, 384:512].astype(bf16).astype(f32)
+    first = at[:entries] % count == 0
+    mid = CMP_STRIDE * HEAD_DIM
+    for branch, inner_weight, outer in ((0, kin, kout_ref), (1, vin, vout_ref)):
+        loads[5 + branch].wait()
+        left, right = [], []
+        for j in range(0, CMP_STRIDE, 2):
+            a = raw[branch, pl.ds(j, entries, stride=CMP_STRIDE), :]
+            b = raw[branch, pl.ds(j + 1, entries, stride=CMP_STRIDE), :]
+            left.append(jnp.where(low_e, a, pltpu.roll(b, HEAD_DIM, 1)))
+            right.append(jnp.where(low_e, pltpu.roll(a, HEAD_DIM, 1), b))
+        window = jnp.concatenate(
+            [jnp.concatenate(left, axis=1), jnp.concatenate(right, axis=1)], axis=0
+        ).astype(bf16)
+        front = dot(window, inner_weight[:mid])
+        back = dot(window, inner_weight[mid:])
+        parts = []
+        for g in range(2):
+            shifted = pltpu.roll(front[g * entries : (g + 1) * entries], 1, 0)
+            parts.append(back[g * entries : (g + 1) * entries] + jnp.where(first, 0.0, shifted))
+        inner = gelu(jnp.concatenate(parts, axis=0)).astype(bf16)
+        outer = jnp.concatenate([outer[...], outer[...]], axis=0)
+        result = dot_t(inner, outer)
+        result = jnp.where(low_e, result[:entries], result[entries:])
+        if branch == 0:
+            result = turn(result, cosine_e, sine_e)
+        start = 2 * span + branch * entries
+        blobs[me, start : start + entries, :] = result.astype(bf16)
+
+    named = jnp.zeros((seqs, 2, TOPK), jnp.int32)
+    for d in range(1, n):
+        origin = (me + d) % n
+        pltpu.make_async_remote_copy(
+            src_ref=picks_ref, dst_ref=lists.at[origin], send_sem=pick_send.at[d - 1],
+            recv_sem=pick_recv.at[origin], device_id={"kv": origin}, device_id_type=mesh_id,
+        ).wait_recv()
+        named = jnp.maximum(named, (lists[origin] == me).astype(jnp.int32))
+    slot_at = lax.broadcasted_iota(jnp.int32, (seqs, 2, TOPK), 2)
+    named = jnp.max(jnp.where(slot_at == 0, 0, named), axis=2, keepdims=True)
+    key = jnp.zeros((span, 128), f32)
+    value = jnp.zeros((span, 128), f32)
+    for s in range(seqs):
+        flag = jnp.where(low, named[s, 0:1, :], named[s, 1:2, :]) > 0
+        key = jnp.where(flag, sk_buf[s * span : (s + 1) * span, :].astype(f32), key)
+        value = jnp.where(flag, sv_buf[s * span : (s + 1) * span, :].astype(f32), value)
+    blobs[me, 0:span, :] = key.astype(bf16)
+    blobs[me, span : 2 * span, :] = value.astype(bf16)
+
+    def pass_on(slot, dst, number):
+        copy = pltpu.make_async_remote_copy(
+            src_ref=blobs.at[slot], dst_ref=blobs.at[slot], send_sem=blob_send.at[number],
+            recv_sem=blob_recv.at[slot], device_id={"kv": dst}, device_id_type=mesh_id,
+        )
+        copy.start()
+        sent.append(copy)
+
+    def arrived(slot):
+        pltpu.make_async_remote_copy(
+            src_ref=blobs.at[slot], dst_ref=blobs.at[slot], send_sem=blob_send.at[0],
+            recv_sem=blob_recv.at[slot], device_id={"kv": (me + 1) % n}, device_id_type=mesh_id,
+        ).wait_recv()
+
+    across = z * PLANE + (1 - x) * 2 + c
+    beside = z * PLANE + x * 2 + (1 - c)
+    order = sorted(range(1, planes), key=lambda d: (min(d, planes - d), d))
+    number = 0
+    for d in order:
+        pass_on(me, ((z + d) % planes) * PLANE + x * 2 + c, number)
+        number += 1
+    pass_on(me, across, number)
+    pass_on(me, beside, number + 1)
+    number += 2
+
+    loads[7].wait()
+    loads[8].wait()
+    hidden = rows[...]
+    for i in range(half):
+        made = dot(hidden, wq[:, i * 128 : (i + 1) * 128])
+        for s in range(seqs):
+            v = turn(made[s * span : (s + 1) * span], cosine, sine) * (HEAD_DIM**-0.5)
+            y = pltpu.roll(v, HEAD_DIM, 1)
+            if 2 * i < half:
+                even, odd = jnp.where(low, v, 0.0), jnp.where(low, y, 0.0)
+            else:
+                even, odd = jnp.where(low, 0.0, y), jnp.where(low, 0.0, v)
+            base = (s * heads + 2 * i) * span
+            q_buf[base : base + span, :] = even.astype(bf16)
+            q_buf[base + span : base + 2 * span, :] = odd.astype(bf16)
+    spread = 2 * wg_ref.shape[1]
+    gate_buf[...] = jnp.zeros_like(gate_buf)
+    gate_buf[:, :spread] = jax.nn.sigmoid(dot_t(hidden, wg[...].reshape(spread, rows.shape[1])))
+
+    for d in order:
+        slot = ((z + planes - d) % planes) * PLANE + x * 2 + c
+        arrived(slot)
+        pass_on(slot, across, number)
+        pass_on(slot, beside, number + 1)
+        number += 2
+    for d in [0] + order:
+        slot = ((z + planes - d) % planes) * PLANE + (1 - x) * 2 + c
+        arrived(slot)
+        pass_on(slot, beside, number)
+        number += 1
+    for d in [0] + order:
+        origin = ((z + planes - d) % planes) * PLANE
+        arrived(origin + x * 2 + (1 - c))
+        arrived(origin + (1 - x) * 2 + (1 - c))
+
+    slot = lax.broadcasted_iota(jnp.int32, (span, n * entries), 1)
+    entry = (slot // entries) * count + slot % count
+    entry_seq = (slot % entries) // count
+    query_at = me * span + lax.broadcasted_iota(jnp.int32, (span, n * entries), 0)
+    entry_ok = (entry >= 1) & (entry * CMP_STRIDE + CMP_STRIDE - 1 <= query_at)
+    row_at = me * span + at
+    far_k = blobs[:, 0:span, :].reshape(far_keys, 128)
+    far_v = blobs[:, span : 2 * span, :].reshape(far_keys, 128)
+    cmp_k = blobs[:, 2 * span : 2 * span + entries, :].reshape(n * entries, 128)
+    cmp_v = blobs[:, 2 * span + entries :, :].reshape(n * entries, 128)
+
+    def piece(s):
+        return pltpu.make_async_remote_copy(
+            src_ref=own.at[s], dst_ref=other.at[s], send_sem=half_send.at[s],
+            recv_sem=half_recv.at[s], device_id={"tp": 1 - column}, device_id_type=mesh_id,
+        )
+
+    def one_sequence(s, carry):
+        part = pl.ds(pl.multiple_of(s * span, span), span)
+        near_k = sk_buf[part, :]
+        near_v = sv_buf[part, :]
+        gates = gate_buf[part, :]
+        gates = jnp.where(column == 0, gates, pltpu.roll(gates, 128 - heads, 1))
+        live = row_at < lens_ref[s]
+        entry_bias = jnp.where(entry_ok & (entry_seq == s), 0.0, FAR)
+        for g in range(2):
+            start = pl.multiple_of((s * heads + g * half) * span, span)
+            q = q_buf[pl.ds(start, half * span), :]
+            sc = dot_t(q, cmp_k).reshape(half, span, n * entries) + entry_bias[None]
+            top = jnp.maximum(jnp.max(sc, axis=-1, keepdims=True), -1e29)
+            e = jnp.exp(sc - top)
+            total = jnp.maximum(jnp.sum(e, axis=-1, keepdims=True), 1.0)
+            w = (e * (1.0 / total)).astype(bf16).reshape(half * span, n * entries)
+            cmp_out = dot(w, cmp_v)
+            sf = dot_t(q, far_k) + bias[s, g : g + 1, :]
+            sn = (dot_t(q, near_k).reshape(half, span, span) + near[...][None]).reshape(
+                half * span, span
+            )
+            top = jnp.maximum(
+                jnp.max(sf, axis=-1, keepdims=True), jnp.max(sn, axis=-1, keepdims=True)
+            )
+            ef = jnp.exp(sf - top)
+            en = jnp.exp(sn - top)
+            total = jnp.sum(ef, axis=-1, keepdims=True) + jnp.sum(en, axis=-1, keepdims=True)
+            inverse = 1.0 / total
+            sel_out = dot((ef * inverse).astype(bf16), far_v) + dot(
+                (en * inverse).astype(bf16), near_v
+            )
+            mixed = []
+            for h in range(half):
+                span_h = slice(h * span, (h + 1) * span)
+                head = g * half + h
+                behind = spread // 2 + head
+                mixed.append(
+                    gates[:, head : head + 1] * cmp_out[span_h]
+                    + gates[:, behind : behind + 1] * sel_out[span_h]
+                )
+            for h in range(0, half, 2):
+                if g == 0:
+                    pair = jnp.where(low, mixed[h], pltpu.roll(mixed[h + 1], HEAD_DIM, 1))
+                else:
+                    pair = jnp.where(low, pltpu.roll(mixed[h], HEAD_DIM, 1), mixed[h + 1])
+                pair = jnp.where(live, pair, 0.0).astype(bf16)
+                lanes = (g * half + h) * HEAD_DIM
+                own[s, :, lanes : lanes + 128] = pair
+        piece(s).start()
+        return carry
+
+    lax.fori_loop(0, seqs, one_sequence, 0)
+    for load in loads[9:]:
+        load.wait()
+    gain_own = gain_ref[:, pl.ds(pl.multiple_of(column * depth, depth), depth)]
+    gain_other = gain_ref[:, pl.ds(pl.multiple_of((1 - column) * depth, depth), depth)]
+
+    def finish(s, carry):
+        piece(s).wait_recv()
+        a = own[s].astype(f32)
+        b = other[s].astype(f32)
+        squares = jnp.sum(a * a, axis=-1, keepdims=True) + jnp.sum(b * b, axis=-1, keepdims=True)
+        row_scale = lax.rsqrt(squares / (2 * depth) + norm_eps)
+        total = dot((a * gain_own).astype(bf16), weight[0]) + dot(
+            (b * gain_other).astype(bf16), weight[1]
+        )
+        out_ref[pl.ds(pl.multiple_of(s * span, span), span), :] = (total * row_scale).astype(bf16)
+        return carry
+
+    lax.fori_loop(0, seqs, finish, 0)
+
+    def close(s, carry):
+        piece(s).wait_send()
+        return carry
+
+    lax.fori_loop(0, seqs, close, 0)
+    for copy in sent:
+        copy.wait_send()
+
+
+def fused_shards(
+    hidden_in,
+    w_query,
+    w_cmp_key,
+    w_cmp_value,
+    w_sel_key,
+    w_sel_value,
+    w_gate,
+    cmp_key_in,
+    cmp_key_out,
+    cmp_value_in,
+    cmp_value_out,
+    out_gain,
+    w_out,
+    seq_lengths,
+    chosen,
+):
+    seqs, span, width = hidden_in.shape
+    n = lax.axis_size("kv")
+    heads = w_query.shape[1] // HEAD_DIM
+    total = seqs * span
+    entries = total // CMP_STRIDE
+    out_width = width // lax.axis_size("tp")
+    small = w_sel_key.shape[1]
+    vmem = pl.BlockSpec(memory_space=pltpu.VMEM)
+    anywhere = pl.BlockSpec(memory_space=pl.ANY)
+    power = jnp.arange(128, dtype=jnp.int32) % (HEAD_DIM // 2) * 2
+    freq = jnp.exp(-jnp.log(f32(theta_base)) * power.astype(f32) / HEAD_DIM)
+    gate_rows = jnp.transpose(w_gate, (1, 2, 0))
+    out = pl.pallas_call(
+        functools.partial(layer_kernel, n, seqs, span, heads),
+        in_specs=[pl.BlockSpec(memory_space=pltpu.SMEM)] + [vmem] * 5 + [anywhere] * 10,
+        out_specs=vmem,
+        out_shape=jax.ShapeDtypeStruct((total, out_width), bf16),
+        scratch_shapes=[
+            pltpu.VMEM((total, width), bf16),
+            pltpu.VMEM(w_query.shape, bf16),
+            pltpu.VMEM((width, 4 * small), bf16),
+            pltpu.VMEM(gate_rows.shape, bf16),
+            pltpu.VMEM(cmp_key_in.shape, bf16),
+            pltpu.VMEM(cmp_value_in.shape, bf16),
+            pltpu.VMEM((2, heads * HEAD_DIM, out_width), bf16),
+            pltpu.VMEM((heads * total, 128), bf16),
+            pltpu.VMEM((total, small), bf16),
+            pltpu.VMEM((total, small), bf16),
+            pltpu.VMEM((2, total, small), f32),
+            pltpu.VMEM((total, 128), f32),
+            pltpu.VMEM((n, seqs, 2, TOPK), jnp.int32),
+            pltpu.VMEM((n, 2 * span + 2 * entries, small), bf16),
+            pltpu.VMEM((seqs, span, heads * HEAD_DIM), bf16),
+            pltpu.VMEM((seqs, span, heads * HEAD_DIM), bf16),
+            pltpu.VMEM((seqs, 2, n * span), f32),
+            pltpu.VMEM((span, span), f32),
+            pltpu.SemaphoreType.DMA((11,)),
+            pltpu.SemaphoreType.DMA((n,)),
+            pltpu.SemaphoreType.DMA((n,)),
+            pltpu.SemaphoreType.DMA((n,)),
+            pltpu.SemaphoreType.DMA((n,)),
+            pltpu.SemaphoreType.DMA((seqs,)),
+            pltpu.SemaphoreType.DMA((seqs,)),
+        ],
+        compiler_params=pltpu.CompilerParams(
+            collective_id=0, has_side_effects=True, vmem_limit_bytes=VMEM_BYTES
+        ),
+        name="layer",
+    )(
+        seq_lengths, chosen[:, 0], freq[None], out_gain[None],
+        jnp.transpose(cmp_key_out), jnp.transpose(cmp_value_out),
+        hidden_in.reshape(total, width), w_query, w_cmp_key, w_cmp_value, w_sel_key,
+        w_sel_value, gate_rows, cmp_key_in, cmp_value_in, w_out,
+    )
+    return out.reshape(seqs, span, out_width)
+
+
+def fits(mesh):
+    n = mesh.shape["kv"]
+    return mesh.shape["tp"] == 2 and n % PLANE == 0 and n <= 32
+
+
 def solution(mesh):
     placed = (
         P(None, "kv", None),
@@ -201,5 +603,5 @@
         P(None, "kv", "tp", None),
     )
     return jax.shard_map(
-        shards, mesh=mesh, in_specs=placed, out_specs=P(None, "kv", "tp"), check_vma=False
-    )
+        fused_shards if fits(mesh) else shards, mesh=mesh, in_specs=placed, out_specs=P(None, "kv", "tp"), check_vma=False
+    )

time: 141 us -> 38.2 us (0.27)
  blocking collectives: 70.7 us -> 0 us
  Pallas kernels: 0 us -> 35.5 us
  local copies, waits for them, and re-layouts: 33.9 us -> 1.87 us
  matrix products: 18.3 us -> 0 us
  other arithmetic: 15.8 us -> 0.52 us
    all_gather x4 -> x0, blocking collectives: 70.7 us -> none  [the longest x1 23.3 us: shards(): every_list = lax.all_gather(picks[None, :, :, 1:], 'kv', axis=0, tiled=True)]
    pallas_call x0 -> x1, Pallas kernels: none -> 35.5 us  [fused_shards(): pl.pallas_call(functools.partial(layer_kernel, n, seqs, span, heads), in_...]
    dot_general x25 -> x0, matrix products: 18.3 us -> none  [the longest x5 6.41 us: project(): jnp.dot(rows, weight_matrix, preferred_element_type=jnp.float32)]
    dynamic_slice x16 -> x0, local copies, waits for them, and re-layouts: 8.72 us -> none  [shards(): lax.map(one_sequence, (queries, remote_entries, picks, sel_pairs, gates,...]
    sub x9 -> x0, other arithmetic: 7.56 us -> none  [the longest x8 7.55 us: masked_weights(): expd = jnp.where(valid, jnp.exp(scores - top), 0.0)]
    unnamed x24 -> x1, local copies, waits for them, and re-layouts: 8.52 us -> 1.87 us
    broadcast_in_dim x16 -> x0, local copies, waits for them, and re-layouts: 5.05 us -> none  [the longest x4 4.28 us: masked_weights(): expd = jnp.where(valid, jnp.exp(scores - top), 0.0)]
    gather x8 -> x0, local copies, waits for them, and re-layouts: 3.25 us -> none  [one_sequence(): table[index]]
where the time goes in v2:
time: 38.2 us; the launch traced here: 37.9 us
  Pallas kernels  35.5 us (93%)
  local copies, waits for them, and re-layouts  1.87 us (5%)
  other arithmetic  0.52 us (1%)
    pallas_call x1, Pallas kernels, fused_shards(): pl.pallas_call(functools.partial(layer_kernel, n, seqs, span, heads), in_...  35.5 us
    unnamed x1, local copies, waits for them, and re-layouts  1.87 us

profile of v2, /device:TPU:0, one launch (start us, length us, event | category | flops | bytes accessed | tf_op | source)
XLA Modules:
  0.0 37.9 jit_solution(778405875068273264)
XLA Ops:
  0.0 0.5 %fusion.3.freq_ref = f32[1,128]{1,0:T(1,128)} fusion(), kind=kLoop, calls=%fused_computation.4 | loop fusion | flops 1152 | bytes 512 | tf_op jit(solution)/shard_map/exp | solution.py:535
  0.5 35.5 %layer.1 = bf16[256,1024]{1,0:T(8,128)(2,1)} custom-call(s32[4]{0:T(128)} %lens_ref.1, s32[4,2,16]{2,1,0:T(2,128)} %bitcast.12, f32[1,128]{1,0:T(1,128)} %fusion.3.freq_ref, f32[1,1024]{1,0:T(1,128)} %bitcast.13, bf16[64,128]{1,0:T(8,128)(2,1)} %bitcast.10, bf16[64,128]{1,0:T(8,128)(2,1)} %bitcast.11, bf16[256,2048]{1,0:T(8,128)(2,1)} %bitcast.8, ...), custom_call_target="tpu_custom_call" | custom-call | tf_op jit(solution)/shard_map/layer/pallas_call | solution.py:537
  36.1 1.9 %copy.17 = bf16[4,64,1024]{2,1,0:T(8,128)(2,1)} copy(bf16[4,64,1024]{2,1,0:T(8,128)(2,1)} %bitcast.7) | data formatting | bytes 1048576

commit v3 on v2

--- a/solution.py
+++ b/solution.py
@@ -1,4 +1,5 @@
 import functools
+import math
 
 import jax
 import jax.numpy as jnp
@@ -217,11 +218,11 @@
 
 def layer_kernel(
     n, seqs, span, heads,
-    lens_ref, picks_ref, freq_ref, gain_ref, kout_ref, vout_ref,
+    lens_ref, picks_ref, gain_ref, kout_ref, vout_ref,
     rows_ref, wq_ref, wck_ref, wcv_ref, wsk_ref, wsv_ref, wg_ref, kin_ref, vin_ref, wout_ref,
     out_ref,
     rows, wq, ws, wg, kin, vin, weight,
-    q_buf, sk_buf, sv_buf, raw, gate_buf, lists, blobs, own, other, bias, near,
+    q_buf, sk_buf, sv_buf, raw, gate_buf, lists, blobs, own, other, bias, near, partial,
     load_sem, pick_send, pick_recv, blob_send, blob_recv, half_send, half_recv,
 ):
     me = lax.axis_index("kv")
@@ -262,11 +263,13 @@
     low_e = low[:entries]
     at = lax.broadcasted_iota(jnp.int32, (span, 128), 0)
     sign = jnp.where(lane % HEAD_DIM < HEAD_DIM // 2, -1.0, 1.0)
-    angle = (me * span + at).astype(f32) * freq_ref[...]
+    power = (lane % (HEAD_DIM // 2) * 2).astype(f32)
+    freq = jnp.exp(-math.log(theta_base) * power / HEAD_DIM)
+    angle = (me * span + at).astype(f32) * freq
     cosine = jnp.cos(angle)
     sine = jnp.sin(angle) * sign
     end = me * span + (at[:entries] % count) * CMP_STRIDE + CMP_STRIDE - 1
-    angle = end.astype(f32) * freq_ref[...]
+    angle = end.astype(f32) * freq[:entries]
     cosine_e = jnp.cos(angle)
     sine_e = jnp.sin(angle) * sign[:entries]
     row_q = lax.broadcasted_iota(jnp.int32, (span, span), 0)
@@ -482,15 +485,19 @@
     gain_own = gain_ref[:, pl.ds(pl.multiple_of(column * depth, depth), depth)]
     gain_other = gain_ref[:, pl.ds(pl.multiple_of((1 - column) * depth, depth), depth)]
 
+    def begin(s, carry):
+        partial[s] = dot((own[s].astype(f32) * gain_own).astype(bf16), weight[0])
+        return carry
+
+    lax.fori_loop(0, seqs, begin, 0)
+
     def finish(s, carry):
         piece(s).wait_recv()
         a = own[s].astype(f32)
         b = other[s].astype(f32)
         squares = jnp.sum(a * a, axis=-1, keepdims=True) + jnp.sum(b * b, axis=-1, keepdims=True)
         row_scale = lax.rsqrt(squares / (2 * depth) + norm_eps)
-        total = dot((a * gain_own).astype(bf16), weight[0]) + dot(
-            (b * gain_other).astype(bf16), weight[1]
-        )
+        total = partial[s] + dot((b * gain_other).astype(bf16), weight[1])
         out_ref[pl.ds(pl.multiple_of(s * span, span), span), :] = (total * row_scale).astype(bf16)
         return carry
 
@@ -531,12 +538,10 @@
     small = w_sel_key.shape[1]
     vmem = pl.BlockSpec(memory_space=pltpu.VMEM)
     anywhere = pl.BlockSpec(memory_space=pl.ANY)
-    power = jnp.arange(128, dtype=jnp.int32) % (HEAD_DIM // 2) * 2
-    freq = jnp.exp(-jnp.log(f32(theta_base)) * power.astype(f32) / HEAD_DIM)
     gate_rows = jnp.transpose(w_gate, (1, 2, 0))
     out = pl.pallas_call(
         functools.partial(layer_kernel, n, seqs, span, heads),
-        in_specs=[pl.BlockSpec(memory_space=pltpu.SMEM)] + [vmem] * 5 + [anywhere] * 10,
+        in_specs=[pl.BlockSpec(memory_space=pltpu.SMEM)] + [vmem] * 4 + [anywhere] * 10,
         out_specs=vmem,
         out_shape=jax.ShapeDtypeStruct((total, out_width), bf16),
         scratch_shapes=[
@@ -558,6 +563,7 @@
             pltpu.VMEM((seqs, span, heads * HEAD_DIM), bf16),
             pltpu.VMEM((seqs, 2, n * span), f32),
             pltpu.VMEM((span, span), f32),
+            pltpu.VMEM((seqs, span, out_width), f32),
             pltpu.SemaphoreType.DMA((11,)),
             pltpu.SemaphoreType.DMA((n,)),
             pltpu.SemaphoreType.DMA((n,)),
@@ -571,7 +577,7 @@
         ),
         name="layer",
     )(
-        seq_lengths, chosen[:, 0], freq[None], out_gain[None],
+        seq_lengths, chosen[:, 0], out_gain[None],
         jnp.transpose(cmp_key_out), jnp.transpose(cmp_value_out),
         hidden_in.reshape(total, width), w_query, w_cmp_key, w_cmp_value, w_sel_key,
         w_sel_value, gate_rows, cmp_key_in, cmp_value_in, w_out,

time: 38.2 us -> 37.5 us (0.982)
  other arithmetic: 0.52 us -> 0 us
    exp x1 -> x0, other arithmetic: 0.52 us -> none  [fused_shards(): freq = jnp.exp(-jnp.log(f32(theta_base)) * power.astype(f32) / HEAD_DIM)]
where the time goes in v3:
time: 37.5 us; the launch traced here: 37.2 us
  Pallas kernels  35.4 us (94%)
  local copies, waits for them, and re-layouts  1.87 us (5%)
    pallas_call x1, Pallas kernels, fused_shards(): pl.pallas_call(functools.partial(layer_kernel, n, seqs, span, heads), in_...  35.4 us
    unnamed x1, local copies, waits for them, and re-layouts  1.87 us

profile of v3, /device:TPU:0, one launch (start us, length us, event | category | flops | bytes accessed | tf_op | source)
XLA Modules:
  0.0 37.2 jit_solution(1865367477580544888)
XLA Ops:
  0.0 35.4 %layer.1 = bf16[256,1024]{1,0:T(8,128)(2,1)} custom-call(s32[4]{0:T(128)} %lens_ref.1, s32[4,2,16]{2,1,0:T(2,128)} %bitcast.12, f32[1,1024]{1,0:T(1,128)} %bitcast.13, bf16[64,128]{1,0:T(8,128)(2,1)} %bitcast.10, bf16[64,128]{1,0:T(8,128)(2,1)} %bitcast.11, bf16[256,2048]{1,0:T(8,128)(2,1)} %bitcast.8, bf16[2048,512]{1,0:T(8,128)(2,1)} %wq_ref.1, ...), custom_call_target="tpu_custom_call" | custom-call | tf_op jit(solution)/shard_map/layer/pallas_call | solution.py:542
  35.4 1.9 %copy.17 = bf16[4,64,1024]{2,1,0:T(8,128)(2,1)} copy(bf16[4,64,1024]{2,1,0:T(8,128)(2,1)} %bitcast.7) | data formatting | bytes 1048576
